TPU v7x, 512 devices: a 8x2x16 block of a 8x8x16 slice. The times are simulated.
512 devices in a mesh: grp: 2 (over y), sp: 32 (over z, core), tp: 8 (over x).
Axes of the slice: x: 8, y: 2, z: 16, core: 2. Of those that a mesh axis runs over, the one named last changes fastest.
The devices are a block of a 8x8x16 slice.
Arguments:
- tokens: bfloat16 [32768, 2048], P(('grp', 'sp'), 'tp'), parts along dimension 0, may hold values from -140 to 140, as said below
- mix_gain: bfloat16 [2, 2048], replicated, may hold values from 0.099609375 to 1.8984375
- gate_weight: bfloat16 [2, 2048, 2048], P(None, 'sp', 'tp'), may hold values from -0.125 to 0.125
- mix_weight: bfloat16 [2, 2048, 2048], P(None, 'sp', 'tp'), may hold values from -0.125 to 0.125
- value_weight: bfloat16 [2, 2048, 2048], P(None, 'sp', 'tp'), may hold values from -0.125 to 0.125
- out_weight: bfloat16 [2, 2048, 2048], P(None, 'sp', 'tp'), may hold values from -0.125 to 0.125
- conv_taps: bfloat16 [2, 3, 2048], P(None, None, 'tp'), may hold values from -3.5 to 3.5
Outputs:
- result_stream: bfloat16 [32768, 2048], P(('grp', 'sp'), 'tp'), parts along dimension 0
There are 2 independent parts, one for each index of `grp`. A program takes and returns all parts, laid end to end along the dimension named above; an argument that names none is the same for every part. Nothing has to cross between parts.
Inputs may be any that keep to these rules, and one draw needn't show every extreme that they name: `tokens`: activations with feature scales of several sizes.
All inputs are finite; a program needn't handle non-finite values.
Results may differ from a plain program's by a relative error of at most 0.015.
Values may be sent and summed in bfloat16 or wider, within the bound.
No kernel may reach another device: no remote copies, remote signals or barrier semaphores. Data moves between devices by JAX's collectives and lax.ppermute only.
A program may use at most 64 MiB of HBM per device.

v0:
```python
import jax
import jax.numpy as jnp
from jax import lax
from jax.sharding import PartitionSpec as P

EPS = 1e-06


def passed_along(x, axis, by):
    devices = lax.axis_size(axis)
    pairs = [(i, i + by) for i in range(devices) if 0 <= i + by < devices]
    return lax.ppermute(x, axis, pairs)


def in_one_piece(arrays, axis, dim, along):
    ends, at = ([], 0)
    for a in arrays[:-1]:
        at += a.shape[along]
        ends.append(at)
    both = jnp.concatenate(arrays, axis=along)
    return tuple(jnp.split(lax.all_gather(both, axis, axis=dim, tiled=True), ends, axis=along))


def in_order(pieces, dim):
    dims = list(pieces.shape[1:])
    dims[dim] *= pieces.shape[0]
    return jnp.moveaxis(pieces, 0, dim).reshape(dims)


def copy_for_each(x, axis):
    copies = jnp.broadcast_to(x, (lax.axis_size(axis), *x.shape))
    return lax.all_to_all(copies, axis, split_axis=0, concat_axis=0, tiled=True)


def collect(x, axis, dim):
    return in_order(copy_for_each(x, axis), dim)


def normed_rows(rows, gain):
    wide_rows = rows.astype(jnp.float32)
    factor = lax.rsqrt(jnp.mean(wide_rows * wide_rows, axis=1, keepdims=True) + EPS)
    return (wide_rows * factor * gain.astype(jnp.float32)).astype(jnp.bfloat16)


def convolve(carried, before, tap_rows):
    padded = jnp.concatenate([before, carried], axis=0)
    row_count = carried.shape[0]
    result = jnp.zeros_like(carried)
    for tap_index in range(tap_rows.shape[0]):
        result = (
            result
            + tap_rows[tap_index].astype(jnp.float32) * padded[tap_index : tap_index + row_count]
        )
    return result


def shards(tokens, mix_gain, gate_weight, mix_weight, value_weight, out_weight, conv_taps):
    layer_count = gate_weight.shape[0]
    conv_reach = conv_taps.shape[1] - 1
    fringe_depth = conv_reach * layer_count
    before_rows = passed_along(tokens[tokens.shape[0] - fringe_depth :], "sp", 1)
    stream = jnp.concatenate([before_rows, tokens], axis=0)
    gathered = in_one_piece((gate_weight, mix_weight, value_weight, out_weight), "sp", 1, 0)
    channels = gate_weight.shape[2]
    for layer_index in range(layer_count):
        whole = collect(stream, "tp", 1)
        normed = normed_rows(whole, mix_gain[layer_index])
        gate = jnp.dot(normed, gathered[0][layer_index], preferred_element_type=jnp.float32)
        inner = jnp.dot(normed, gathered[1][layer_index], preferred_element_type=jnp.float32)
        values = jnp.dot(normed, gathered[2][layer_index], preferred_element_type=jnp.float32)
        gate = gate.astype(jnp.bfloat16)
        inner = inner.astype(jnp.bfloat16)
        values = values.astype(jnp.bfloat16)
        carried = inner.astype(jnp.float32) * values.astype(jnp.float32)
        before = jnp.zeros((conv_reach, channels), jnp.float32)
        conv = convolve(carried, before, conv_taps[layer_index])
        mixed = (gate.astype(jnp.float32) * conv).astype(jnp.bfloat16)
        mixed_all = lax.all_gather(mixed, "tp", axis=1, tiled=True)
        product = jnp.dot(mixed_all, gathered[3][layer_index], preferred_element_type=jnp.float32)
        stream = (stream.astype(jnp.float32) + product).astype(jnp.bfloat16)
    return stream[fringe_depth:]


def solution(mesh):
    return jax.shard_map(
        shards,
        mesh=mesh,
        in_specs=(
            P(("grp", "sp"), "tp"),
            P(),
            P(None, "sp", "tp"),
            P(None, "sp", "tp"),
            P(None, "sp", "tp"),
            P(None, "sp", "tp"),
            P(None, None, "tp"),
        ),
        out_specs=P(("grp", "sp"), "tp"),
        check_vma=False,
    )
```

profile of v0, /device:TPU:66, one launch (start us, length us, event | category | flops | bytes accessed | tf_op | source)
XLA Modules:
  0.0 306.0 jit_solution(15098368979078359198)
XLA Ops:
  6.6 1.7 pad_maximum_fusion.1
  8.3 0.7 slice.88
  9.0 1.8 collective-permute-start
  10.8 0.8 collective-permute-done
  11.6 1.0 pad_maximum_fusion
  12.6 1.5 broadcast_in_dim.4
  14.1 43.5 %all-to-all-start = ((bf16[8,516,256]{2,1,0:T(8,128)(2,1)}), bf16[8,516,256]{2,1,0:T(8,128)(2,1)S(1)}, u32[]{:S(2)}, u32[]{:S(2)}) async-start(bf16[8,516,256]{2,1,0:T(8,128)(2,1)} %broadcast_in_dim.4), calls=%async_computation | async-start | bytes 4259840 | tf_op jit(solution)/shard_map/all_to_all | solution.py:32
  57.8 51.2 %all-to-all-done = bf16[8,516,256]{2,1,0:T(8,128)(2,1)S(1)} async-done(((bf16[8,516,256]{2,1,0:T(8,128)(2,1)}), bf16[8,516,256]{2,1,0:T(8,128)(2,1)S(1)}, u32[]{:S(2)}, u32[]{:S(2)}) %all-to-all-start) | async-done | bytes 2113568 | tf_op jit(solution)/shard_map/all_to_all | solution.py:32
  109.0 0.5 fusion
  109.5 0.6 fusion.7
  110.0 0.4 copy.8
  110.5 0.1 pad.8
  110.6 0.7 copy.10
  111.3 12.6 %all-gather.4.cloned.1.call-done = bf16[8,2048,256]{2,1,0:T(8,128)(2,1)} async-done(((bf16[8,64,256]{2,1,0:T(8,128)(2,1)}), bf16[8,2048,256]{2,1,0:T(8,128)(2,1)}) %all-gather.4.cloned.1.call-update) | async-done | bytes 8388624 | tf_op jit(solution)/shard_map/all_gather | solution.py:21
  123.9 2.0 fusion.13
  125.9 2.0 fusion.12
  128.0 2.7 fusion.10
  130.8 49.9 %all-gather.6.cloned.1.call-done = bf16[516,2048]{1,0:T(8,128)(2,1)} async-done(((bf16[516,256]{1,0:T(8,128)(2,1)}), bf16[516,2048]{1,0:T(8,128)(2,1)}) %all-gather.6.cloned.1.call-update) | async-done | bytes 2113552 | tf_op jit(solution)/shard_map/all_gather | solution.py:78
  180.7 2.6 add_convert_fusion
  183.3 1.5 broadcast_in_dim.5
  184.8 5.6 %all-to-all-start.1 = ((bf16[8,516,256]{2,1,0:T(8,128)(2,1)}), bf16[8,516,256]{2,1,0:T(8,128)(2,1)S(1)}, u32[]{:S(2)}, u32[]{:S(2)}) async-start(bf16[8,516,256]{2,1,0:T(8,128)(2,1)} %broadcast_in_dim.5), calls=%async_computation.1 | async-start | bytes 4259840 | tf_op jit(solution)/shard_map/all_to_all | solution.py:32
  190.3 45.0 %all-to-all-done.1 = bf16[8,516,256]{2,1,0:T(8,128)(2,1)S(1)} async-done(((bf16[8,516,256]{2,1,0:T(8,128)(2,1)}), bf16[8,516,256]{2,1,0:T(8,128)(2,1)S(1)}, u32[]{:S(2)}, u32[]{:S(2)}) %all-to-all-start.1) | async-done | bytes 2113568 | tf_op jit(solution)/shard_map/all_to_all | solution.py:32
  235.3 0.5 fusion.3
  235.9 0.6 fusion.6
  236.4 0.4 copy.9
  237.0 0.7 copy.11
  237.7 2.0 fusion.19
  239.7 2.0 fusion.18
  241.7 2.7 fusion.16
  244.5 51.6 %all-gather.8.cloned.1.call-done = bf16[516,2048]{1,0:T(8,128)(2,1)} async-done(((bf16[516,256]{1,0:T(8,128)(2,1)}), bf16[516,2048]{1,0:T(8,128)(2,1)}) %all-gather.8.cloned.1.call-update) | async-done | bytes 2113552 | tf_op jit(solution)/shard_map/all_gather | solution.py:78
  296.0 2.6 fusion.20
  298.6 0.8 fusion.22
  (19 shorter events, 0.4 us)
Async XLA Ops:
  6.5 117.4 %all-gather.4.cloned.1.call-start = ((), (), s32[]{:S(2)}) async-start(), calls=%async_computation.2 | async-start | bytes 8650752 | tf_op jit(solution)/shard_map/all_gather | solution.py:21
  9.0 2.6 collective-permute-start
  14.1 43.5 %copy-start.1 = (bf16[2,2048]{1,0:T(2,128)(2,1)S(1)}, bf16[2,2048]{1,0:T(2,128)(2,1)}, u32[]{:S(2)}) copy-start(bf16[2,2048]{1,0:T(2,128)(2,1)} %param.8) | copy-start | bytes 24580
  14.1 43.6 %copy-start.2 = (bf16[2,3,256]{2,0,1:T(2,128)(2,1)S(1)}, bf16[2,3,256]{2,0,1:T(2,128)(2,1)}, u32[]{:S(2)}) copy-start(bf16[2,3,256]{2,0,1:T(2,128)(2,1)} %param.13) | copy-start | bytes 9220
  14.1 94.8 %all-to-all-start = ((bf16[8,516,256]{2,1,0:T(8,128)(2,1)}), bf16[8,516,256]{2,1,0:T(8,128)(2,1)S(1)}, u32[]{:S(2)}, u32[]{:S(2)}) async-start(bf16[8,516,256]{2,1,0:T(8,128)(2,1)} %broadcast_in_dim.4), calls=%async_computation | async-start | bytes 4259840 | tf_op jit(solution)/shard_map/all_to_all | solution.py:32
  57.7 123.0 %all-gather.6.cloned.1.call-start = ((), (), s32[]{:S(2)}) async-start(), calls=%async_computation.3 | async-start | bytes 2396160 | tf_op jit(solution)/shard_map/all_gather | solution.py:78
  127.9 52.7 %copy-start = (bf16[512,256]{1,0:T(8,128)(2,1)S(1)}, bf16[512,256]{1,0:T(8,128)(2,1)}, u32[]{:S(2)}) copy-start(bf16[512,256]{1,0:T(8,128)(2,1)} %param.7) | copy-start | bytes 786436
  184.8 50.6 %all-to-all-start.1 = ((bf16[8,516,256]{2,1,0:T(8,128)(2,1)}), bf16[8,516,256]{2,1,0:T(8,128)(2,1)S(1)}, u32[]{:S(2)}, u32[]{:S(2)}) async-start(bf16[8,516,256]{2,1,0:T(8,128)(2,1)} %broadcast_in_dim.5), calls=%async_computation.1 | async-start | bytes 4259840 | tf_op jit(solution)/shard_map/all_to_all | solution.py:32
  190.3 105.7 %all-gather.8.cloned.1.call-start = ((), (), s32[]{:S(2)}) async-start(), calls=%async_computation.4 | async-start | bytes 2396160 | tf_op jit(solution)/shard_map/all_gather | solution.py:78
Sparse Core Ops, SparseCore 0:
  9.5 114.3 all-gather.3
  130.9 49.7 all-gather.5
  244.6 51.3 all-gather.7
where the time goes:
time: 307 us; the launch traced here: 306 us
  waiting for transfers between devices  211 us (69%)
  starting transfers between devices  50.9 us (17%)
  matrix products  18.6 us (6%)
  between operations  13.3 us (4%)
  local copies, waits for them, and re-layouts  6.28 us (2%)
  other arithmetic  5.67 us (2%)
    all_gather x2, waiting for transfers between devices, shards(): mixed_all = lax.all_gather(mixed, 'tp', axis=1, tiled=True)  101 us
    all_to_all x2, waiting for transfers between devices, copy_for_each(): return lax.all_to_all(copies, axis, split_axis=0, concat_axis=0, tiled=True)  96.2 us
    all_to_all x2, starting transfers between devices, copy_for_each(): return lax.all_to_all(copies, axis, split_axis=0, concat_axis=0, tiled=True)  49.1 us
    all_gather x1, waiting for transfers between devices, in_one_piece(): lax.all_gather(both, axis, axis=dim, tiled=True)  12.6 us
  transfers between devices with their start and end apart: 6, of which 6 were waited for; matrix products, arithmetic and copies ran while one was open for 2% of the time, Pallas kernels for 0%

commit v1 on v0

--- a/solution.py
+++ b/solution.py
@@ -2,6 +2,7 @@
 import jax.numpy as jnp
 from jax import lax
 from jax.sharding import PartitionSpec as P
+from jax.lax import all_to_all, axis_size
 
 EPS = 1e-06
 
@@ -75,7 +76,12 @@
         before = jnp.zeros((conv_reach, channels), jnp.float32)
         conv = convolve(carried, before, conv_taps[layer_index])
         mixed = (gate.astype(jnp.float32) * conv).astype(jnp.bfloat16)
-        mixed_all = lax.all_gather(mixed, "tp", axis=1, tiled=True)
+        mixed_all = jnp.concatenate(
+            all_to_all(
+                jnp.stack([mixed] * axis_size("tp")), axis_name="tp", split_axis=0, concat_axis=0
+            ),
+            1,
+        )
         product = jnp.dot(mixed_all, gathered[3][layer_index], preferred_element_type=jnp.float32)
         stream = (stream.astype(jnp.float32) + product).astype(jnp.bfloat16)
     return stream[fringe_depth:]

time: 307 us -> 322 us (1.049)
  the two profiles are of different devices: /device:TPU:66 before, /device:TPU:65 now
where the time goes in v1:
time: 322 us; the launch traced here: 321 us
  waiting for transfers between devices  152 us (47%)
  blocking collectives  112 us (35%)
  starting transfers between devices  15 us (5%)
  between operations  13.7 us (4%)
  local copies, waits for them, and re-layouts  11.1 us (3%)
  matrix products  11 us (3%)
  other arithmetic  5.67 us (2%)
    all_to_all x2, blocking collectives, shards(): all_to_all(jnp.stack([mixed] * axis_size('tp')), axis_name='tp', split_ax...  112 us
    all_to_all x2, waiting for transfers between devices, copy_for_each(): return lax.all_to_all(copies, axis, split_axis=0, concat_axis=0, tiled=True)  101 us
    ppermute x1, waiting for transfers between devices, passed_along(): return lax.ppermute(x, axis, pairs)  36.3 us
    all_gather x1, waiting for transfers between devices, in_one_piece(): lax.all_gather(both, axis, axis=dim, tiled=True)  15.4 us
    all_to_all x2, starting transfers between devices, copy_for_each(): return lax.all_to_all(copies, axis, split_axis=0, concat_axis=0, tiled=True)  7.93 us
    ppermute x1, starting transfers between devices, passed_along(): return lax.ppermute(x, axis, pairs)  7.05 us
  transfers between devices with their start and end apart: 4, of which 4 were waited for; matrix products, arithmetic and copies ran while one was open for 2% of the time, Pallas kernels for 0%

profile of v1, /device:TPU:65, one launch (start us, length us, event | category | flops | bytes accessed | tf_op | source)
XLA Modules:
  0.0 320.9 jit_solution(4269674332909985425)
XLA Ops:
  6.6 1.7 pad_maximum_fusion.1
  8.3 0.7 slice.88
  9.0 7.0 %collective-permute-start = (bf16[4,256]{1,0:T(4,128)(2,1)S(1)}, bf16[4,256]{1,0:T(4,128)(2,1)S(1)}, u32[]{:S(2)}, u32[]{:S(2)}) collective-permute-start(bf16[4,256]{1,0:T(4,128)(2,1)S(1)} %slice.88), channel_id=1, source_target_pairs={{0,8},{8,16},{16,24},{24,32},{32,40},{40,48},{48,56},{56,64},{64,7... | collective-permute-start | bytes 6152 | tf_op jit(solution)/shard_map/ppermute | solution.py:13
  16.0 36.3 %collective-permute-done = bf16[4,256]{1,0:T(4,128)(2,1)S(1)} collective-permute-done((bf16[4,256]{1,0:T(4,128)(2,1)S(1)}, bf16[4,256]{1,0:T(4,128)(2,1)S(1)}, u32[]{:S(2)}, u32[]{:S(2)}) %collective-permute-start) | collective-permute-done | bytes 2080 | tf_op jit(solution)/shard_map/ppermute | solution.py:13
  52.3 1.0 pad_maximum_fusion
  53.4 1.5 broadcast_in_dim.4
  54.9 3.9 %all-to-all-start = ((bf16[8,516,256]{2,1,0:T(8,128)(2,1)}), bf16[8,516,256]{2,1,0:T(8,128)(2,1)S(1)}, u32[]{:S(2)}, u32[]{:S(2)}) async-start(bf16[8,516,256]{2,1,0:T(8,128)(2,1)} %broadcast_in_dim.4), calls=%async_computation | async-start | bytes 4259840 | tf_op jit(solution)/shard_map/all_to_all | solution.py:33
  58.9 48.7 %all-to-all-done = bf16[8,516,256]{2,1,0:T(8,128)(2,1)S(1)} async-done(((bf16[8,516,256]{2,1,0:T(8,128)(2,1)}), bf16[8,516,256]{2,1,0:T(8,128)(2,1)S(1)}, u32[]{:S(2)}, u32[]{:S(2)}) %all-to-all-start) | async-done | bytes 2113568 | tf_op jit(solution)/shard_map/all_to_all | solution.py:33
  107.6 0.5 fusion
  108.1 0.6 fusion.7
  109.2 0.7 copy.12
  110.0 15.4 %all-gather.2.cloned.1.call-done = bf16[8,2048,256]{2,1,0:T(8,128)(2,1)} async-done(((bf16[8,64,256]{2,1,0:T(8,128)(2,1)}), bf16[8,2048,256]{2,1,0:T(8,128)(2,1)}) %all-gather.2.cloned.1.call-update) | async-done | bytes 8388624 | tf_op jit(solution)/shard_map/all_gather | solution.py:22
  125.3 2.0 fusion.13
  127.3 2.0 fusion.12
  129.3 2.0 fusion.10
  131.5 57.8 %all_to_all.20 = bf16[8,516,256]{2,1,0:T(8,128)(2,1)S(1)} all-to-all(bf16[8,516,256]{2,1,0:T(8,128)(2,1)S(1)} %stack.4), channel_id=1, replica_groups=mesh['grp'=2,'sp'=32,'tp'=8] {'tp'}, dimensions={0} | all-to-all | bytes 4227072 | tf_op jit(solution)/shard_map/all_to_all | solution.py:80
  189.8 0.7 copy.13
  190.7 2.0 add_convert_fusion
  192.7 1.5 broadcast_in_dim.5
  194.2 4.0 %all-to-all-start.2 = ((bf16[8,516,256]{2,1,0:T(8,128)(2,1)}), bf16[8,516,256]{2,1,0:T(8,128)(2,1)S(1)}, u32[]{:S(2)}, u32[]{:S(2)}) async-start(bf16[8,516,256]{2,1,0:T(8,128)(2,1)} %broadcast_in_dim.5), calls=%async_computation.2 | async-start | bytes 4259840 | tf_op jit(solution)/shard_map/all_to_all | solution.py:33
  198.2 52.1 %all-to-all-done.2 = bf16[8,516,256]{2,1,0:T(8,128)(2,1)S(1)} async-done(((bf16[8,516,256]{2,1,0:T(8,128)(2,1)}), bf16[8,516,256]{2,1,0:T(8,128)(2,1)S(1)}, u32[]{:S(2)}, u32[]{:S(2)}) %all-to-all-start.2) | async-done | bytes 2113568 | tf_op jit(solution)/shard_map/all_to_all | solution.py:33
  250.3 0.5 fusion.3
  250.8 0.5 fusion.6
  252.0 0.7 copy.14
  253.0 1.4 slice-done.1
  254.4 0.8 fusion.19
  255.2 0.8 fusion.18
  256.0 0.8 fusion.16
  256.9 54.2 %all_to_all.21 = bf16[8,516,256]{2,1,0:T(8,128)(2,1)S(1)} all-to-all(bf16[8,516,256]{2,1,0:T(8,128)(2,1)S(1)} %stack.5), channel_id=1, replica_groups=mesh['grp'=2,'sp'=32,'tp'=8] {'tp'}, dimensions={0} | all-to-all | bytes 4227072 | tf_op jit(solution)/shard_map/all_to_all | solution.py:80
  311.7 0.7 copy.15
  312.4 0.8 fusion.20
  313.2 0.8 fusion.22
  (28 shorter events, 3.2 us)
Async XLA Ops:
  6.5 118.8 %all-gather.2.cloned.1.call-start = ((), (), s32[]{:S(2)}) async-start(), calls=%async_computation.4 | async-start | bytes 8650752 | tf_op jit(solution)/shard_map/all_gather | solution.py:22
  9.0 43.4 %collective-permute-start = (bf16[4,256]{1,0:T(4,128)(2,1)S(1)}, bf16[4,256]{1,0:T(4,128)(2,1)S(1)}, u32[]{:S(2)}, u32[]{:S(2)}) collective-permute-start(bf16[4,256]{1,0:T(4,128)(2,1)S(1)} %slice.88), channel_id=1, source_target_pairs={{0,8},{8,16},{16,24},{24,32},{32,40},{40,48},{48,56},{56,64},{64,7... | collective-permute-start | bytes 6152 | tf_op jit(solution)/shard_map/ppermute | solution.py:13
  54.9 4.0 %copy-start.1 = (bf16[2,2048]{1,0:T(2,128)(2,1)S(1)}, bf16[2,2048]{1,0:T(2,128)(2,1)}, u32[]{:S(2)}) copy-start(bf16[2,2048]{1,0:T(2,128)(2,1)} %param.8) | copy-start | bytes 24580
  54.9 4.0 %copy-start.2 = (bf16[2,3,256]{2,0,1:T(2,128)(2,1)S(1)}, bf16[2,3,256]{2,0,1:T(2,128)(2,1)}, u32[]{:S(2)}) copy-start(bf16[2,3,256]{2,0,1:T(2,128)(2,1)} %param.13) | copy-start | bytes 9220
  54.9 52.7 %all-to-all-start = ((bf16[8,516,256]{2,1,0:T(8,128)(2,1)}), bf16[8,516,256]{2,1,0:T(8,128)(2,1)S(1)}, u32[]{:S(2)}, u32[]{:S(2)}) async-start(bf16[8,516,256]{2,1,0:T(8,128)(2,1)} %broadcast_in_dim.4), calls=%async_computation | async-start | bytes 4259840 | tf_op jit(solution)/shard_map/all_to_all | solution.py:33
  189.8 1.0 copy-start
  194.2 56.1 %all-to-all-start.2 = ((bf16[8,516,256]{2,1,0:T(8,128)(2,1)}), bf16[8,516,256]{2,1,0:T(8,128)(2,1)S(1)}, u32[]{:S(2)}, u32[]{:S(2)}) async-start(bf16[8,516,256]{2,1,0:T(8,128)(2,1)} %broadcast_in_dim.5), calls=%async_computation.2 | async-start | bytes 4259840 | tf_op jit(solution)/shard_map/all_to_all | solution.py:33
  250.8 2.2 slice-start
  251.4 3.0 slice-start.1
Sparse Core Ops, SparseCore 0:
  9.5 115.7 all-gather.1
